TPU v7x, 512 devices: a whole 4x4x16 slice. The times are simulated.
512 devices in a mesh: rep: 2 (over z_hi), fs: 32 (over z_lo, y), tp: 8 (over x, core).
Axes of the slice: x: 4, y: 4, z: 16 (z_hi: 2, z_lo: 8; z = z_hi * 8 + z_lo), core: 2. Of those that a mesh axis runs over, the one named last changes fastest.
Arguments:
- tokens: bfloat16 [64, 1024, 1024], P(('rep', 'fs'), 'tp'), may hold values from -6 to 6
- mixer_in_gain: float32 [1024], replicated, may hold values from 0.5 to 1.5
- query_weight: bfloat16 [1024, 1024], P('fs', 'tp'), may hold values from -0.1875 to 0.1875
- key_weight: bfloat16 [1024, 1024], P('fs', 'tp'), may hold values from -0.1875 to 0.1875
- value_weight: bfloat16 [1024, 2048], P('fs', 'tp'), may hold values from -0.1875 to 0.1875
- gate_weight: bfloat16 [1024, 2048], P('fs', 'tp'), may hold values from -0.1875 to 0.1875
- decay_logits: float32 [2, 8], P(None, 'tp'), may hold values from 3.4 to 6.2
- mixer_output: bfloat16 [2048, 1024], P('tp', 'fs'), may hold values from -0.125 to 0.125
- mixer_out_gain: float32 [1024], replicated, may hold values from 0.5 to 1.5
- channel_in_gain: float32 [1024], replicated, may hold values from 0.5 to 1.5
- gelu_weight: bfloat16 [1024, 2816], P('fs', 'tp'), may hold values from -0.1875 to 0.1875
- linear_weight: bfloat16 [1024, 2816], P('fs', 'tp'), may hold values from -0.1875 to 0.1875
- gelu_kernel: float32 [3, 2816], P(None, 'tp'), may hold values from -3.5 to 3.5
- linear_kernel: float32 [3, 2816], P(None, 'tp'), may hold values from -3.5 to 3.5
- gelu_bias: float32 [2816], P('tp'), may hold values from -1.2 to 1.2
- linear_bias: float32 [2816], P('tp'), may hold values from -1.2 to 1.2
- down_weight: bfloat16 [2816, 1024], P('tp', 'fs'), may hold values from -0.109375 to 0.109375
- channel_out_gain: float32 [1024], replicated, may hold values from 0.5 to 1.5
Outputs:
- layer_output: bfloat16 [64, 1024, 1024], P(('rep', 'fs'), 'tp')
All inputs are finite; a program needn't handle non-finite values.
Results may differ from a plain program's by a relative error of at most 0.02.
Values may be sent and summed in bfloat16 or wider, within the bound.
No kernel may reach another device: no remote copies, remote signals or barrier semaphores. Data moves between devices by JAX's collectives and lax.ppermute only.
A program may use at most 64 MiB of HBM per device.

v0:
```python
import jax
import jax.numpy as jnp
from jax import lax
from jax.sharding import Mesh
from jax.sharding import PartitionSpec as P

DK = 128
DV = 256
SPAN = 128
TP = ("tp_0", "tp_1")
epsilon = 1e-06
rope_base = 10000.0


def joined_along(pieces, dim):
    lengths = list(pieces.shape[1:])
    lengths[dim] *= pieces.shape[0]
    return jnp.moveaxis(pieces, 0, dim).reshape(lengths)


def gather_together(arrays, axis, dims):
    flat = jnp.concatenate([a.reshape(-1) for a in arrays])
    lines, at, gathered = (lax.all_gather(flat, axis), 0, [])
    for a, dim in zip(arrays, dims):
        pieces = lines[:, at : at + a.size].reshape(-1, *a.shape)
        gathered.append(joined_along(pieces, dim))
        at += a.size
    return tuple(gathered)


def piece_ends(length, count):
    unit = 8 if length >= 8 * count else 1
    return [length // unit * k // count * unit for k in range(1, count)]


def all_blocks(value, axes, order):
    pieces = value[None]
    for k in order:
        pieces = lax.all_gather(pieces, axes[k], axis=0, tiled=True)
    carried = [lax.axis_size(axes[k]) for k in reversed(order)]
    pieces = pieces.reshape(*carried, *value.shape)
    turned = sorted(range(len(order)), key=lambda place: order[len(order) - 1 - place])
    return pieces.transpose(*turned, *range(len(order), pieces.ndim)).reshape(-1, *value.shape)


def gather_at_once(value, axes, dim):
    cut = max(range(max(1, value.ndim - 1)), key=lambda d: value.shape[d])
    count, gathered = (len(axes), [])
    for leading, piece in enumerate(
        jnp.split(value, piece_ends(value.shape[cut], count), axis=cut)
    ):
        if piece.size:
            order = [(leading - k) % count for k in range(count)]
            gathered.append(all_blocks(piece, axes, order))
    return joined_along(jnp.concatenate(gathered, axis=cut + 1), dim)


def on_whole(value, axes, dim, work):
    everything = gather_at_once(value, axes, dim)
    return work(everything, jnp.int32(0))


def own_rows_2(product, extent, axis):
    everything = product(jnp.int32(0), lax.axis_size(axis) * extent)
    own = lax.psum_scatter(everything.astype(jnp.bfloat16), axis, scatter_dimension=0, tiled=True)
    return own.astype(jnp.float32)


def rms_scaled(row_values, norm_gain):
    values = row_values.astype(jnp.float32)
    return (
        values * lax.rsqrt(jnp.mean(values * values, axis=-1, keepdims=True) + epsilon) * norm_gain
    )


def rotate(values, positions):
    half_width = values.shape[-1] // 2
    frequency = 1.0 / rope_base ** (jnp.arange(half_width, dtype=jnp.float32) / half_width)
    angles = positions.astype(jnp.float32)[:, None] * frequency[None, :]
    cosine = jnp.cos(angles)[:, None, :]
    sine_part = jnp.sin(angles)[:, None, :]
    first_half = values[..., :half_width]
    second = values[..., half_width:]
    return jnp.concatenate(
        [first_half * cosine - second * sine_part, first_half * sine_part + second * cosine],
        axis=-1,
    )


def one_direction(queries, key_rows, value_rows, log_decay, strict):
    highest = lax.Precision.HIGHEST
    length = queries.shape[0]
    head_count = queries.shape[1]
    block_count = length // SPAN
    inside_index = jnp.arange(SPAN, dtype=jnp.float32)
    offset = inside_index[:, None] - inside_index[None, :]
    allowed = offset >= (1.0 if strict else 0.0)
    within = jnp.where(
        allowed[None],
        jnp.exp(jnp.where(allowed, offset, 0.0)[None] * log_decay[:, None, None]),
        0.0,
    )
    query_blocks = queries.reshape(block_count, SPAN, head_count, -1)
    key_blocks = key_rows.reshape(block_count, SPAN, head_count, -1)
    value_blocks = value_rows.reshape(block_count, SPAN, head_count, -1).astype(jnp.float32)
    scores = (
        jnp.einsum("nchd,nmhd->nhcm", query_blocks, key_blocks, preferred_element_type=jnp.float32)
        * within[None]
    )
    inside = jnp.einsum("nhcm,nmhe->nche", scores, value_blocks, precision=highest)
    tail_decay = jnp.exp((SPAN - 1.0 - inside_index)[:, None] * log_decay[None, :])
    lead_decay = jnp.exp((inside_index + 1.0)[:, None] * log_decay[None, :])
    step_decay = jnp.exp(SPAN * log_decay)
    updates = jnp.einsum(
        "nmhd,nmhe->nhde",
        key_blocks.astype(jnp.float32),
        value_blocks * tail_decay[None, :, :, None],
        precision=highest,
    )

    def advance(carried, update):
        return (step_decay[:, None, None] * carried + update, carried)

    _, before = lax.scan(advance, jnp.zeros(updates.shape[1:], jnp.float32), updates)
    across = jnp.einsum(
        "nchd,nhde->nche",
        query_blocks.astype(jnp.float32) * lead_decay[None, :, :, None],
        before,
        precision=highest,
    )
    return (inside + across).reshape(length, head_count, -1)


def retention(queries, key_rows, value_rows, logits):
    log_forward = jax.nn.log_sigmoid(logits[0])
    log_backward = jax.nn.log_sigmoid(logits[1])
    forward = one_direction(queries, key_rows, value_rows, log_forward, False)
    behind = one_direction(queries[::-1], key_rows[::-1], value_rows[::-1], log_backward, True)[
        ::-1
    ]
    return forward + behind


def head_norm(values):
    centred = values - jnp.mean(values, axis=-1, keepdims=True)
    return centred * lax.rsqrt(jnp.mean(centred * centred, axis=-1, keepdims=True) + epsilon)


def conv_positions(values, kernel, biases):
    padded = jnp.pad(values.astype(jnp.float32), ((1, 1), (0, 0)))
    return kernel[0] * padded[:-2] + kernel[1] * padded[1:-1] + kernel[2] * padded[2:] + biases


def per_device(
    tokens,
    mixer_in_gain,
    query_weight,
    key_weight,
    value_weight,
    gate_weight,
    decay_logits,
    mixer_output,
    mixer_out_gain,
    channel_in_gain,
    gelu_weight,
    linear_weight,
    gelu_kernel,
    linear_kernel,
    gelu_bias,
    linear_bias,
    down_weight,
    channel_out_gain,
):
    token_rows = tokens[0]
    own_rows = token_rows.shape[0]
    normed = rms_scaled(token_rows, mixer_in_gain).astype(jnp.bfloat16)
    query_full, key_full, value_full, gate_full = gather_together(
        (query_weight, key_weight, value_weight, gate_weight), "fs", (0, 0, 0, 0)
    )
    query_width = query_full.shape[1]
    value_width = value_full.shape[1]
    head_count = query_width // DK

    def project(row_block, first_row):
        row_total = row_block.shape[0]
        positions = first_row + jnp.arange(row_total, dtype=jnp.int32)
        query_raw = jnp.dot(row_block, query_full, preferred_element_type=jnp.float32).reshape(
            row_total, head_count, DK
        )
        query_part = rotate(query_raw, positions).reshape(row_total, query_width)
        key_raw = jnp.dot(row_block, key_full, preferred_element_type=jnp.float32).reshape(
            row_total, head_count, DK
        )
        key_part = (rotate(key_raw, positions) * DK ** (-0.5)).reshape(row_total, query_width)
        value_part = jnp.dot(row_block, value_full, preferred_element_type=jnp.float32)
        gate_part = jnp.dot(row_block, gate_full, preferred_element_type=jnp.float32)
        return jnp.concatenate([query_part, key_part, value_part, gate_part], axis=1).astype(
            jnp.bfloat16
        )

    joined = on_whole(normed, TP, 0, project)
    length = joined.shape[0]
    queries = joined[:, :query_width].reshape(length, head_count, DK)
    key_rows = joined[:, query_width : 2 * query_width].reshape(length, head_count, DK)
    value_rows = joined[:, 2 * query_width : 2 * query_width + value_width].reshape(
        length, head_count, DV
    )
    gate_rows = joined[:, 2 * query_width + value_width :]
    retained = retention(queries, key_rows, value_rows, decay_logits)
    gated = (
        head_norm(retained).reshape(length, value_width)
        * jax.nn.silu(gate_rows.astype(jnp.float32))
    ).astype(jnp.bfloat16)
    output_columns = lax.all_gather(mixer_output, "fs", axis=1, tiled=True)

    def mixer_term(first_row, row_count):
        row_part = lax.dynamic_slice_in_dim(gated, first_row, row_count, 0)
        return jnp.dot(row_part, output_columns, preferred_element_type=jnp.float32)

    mix_sum = own_rows_2(mixer_term, own_rows, TP)
    after_mix = (token_rows.astype(jnp.float32) + rms_scaled(mix_sum, mixer_out_gain)).astype(
        jnp.bfloat16
    )
    channel_in = rms_scaled(after_mix, channel_in_gain).astype(jnp.bfloat16)
    gelu_full, linear_full = gather_together((gelu_weight, linear_weight), "fs", (0, 0))

    def expand(row_block, first_row):
        gelu_part = jnp.dot(row_block, gelu_full, preferred_element_type=jnp.float32)
        linear_part = jnp.dot(row_block, linear_full, preferred_element_type=jnp.float32)
        return jnp.concatenate([gelu_part, linear_part], axis=1).astype(jnp.bfloat16)

    both_parts = on_whole(channel_in, TP, 0, expand)
    gelu_in = both_parts[:, : gelu_full.shape[1]]
    linear_in = both_parts[:, gelu_full.shape[1] :]
    hidden = (
        jax.nn.gelu(conv_positions(gelu_in, gelu_kernel, gelu_bias))
        * conv_positions(linear_in, linear_kernel, linear_bias)
    ).astype(jnp.bfloat16)
    down_columns = lax.all_gather(down_weight, "fs", axis=1, tiled=True)

    def channel_term(first_row, row_count):
        row_part = lax.dynamic_slice_in_dim(hidden, first_row, row_count, 0)
        return jnp.dot(row_part, down_columns, preferred_element_type=jnp.float32)

    channel_sum = own_rows_2(channel_term, own_rows, TP)
    result = (after_mix.astype(jnp.float32) + rms_scaled(channel_sum, channel_out_gain)).astype(
        jnp.bfloat16
    )
    return result[None]


def solution(mesh):
    split = Mesh(
        mesh.devices.reshape(mesh.shape["rep"], mesh.shape["fs"], 4, 2),
        ("rep", "fs", "tp_0", "tp_1"),
    )
    in_specs = (
        P(("rep", "fs"), TP, None),
        P(),
        P("fs", TP),
        P("fs", TP),
        P("fs", TP),
        P("fs", TP),
        P(None, TP),
        P(TP, "fs"),
        P(),
        P(),
        P("fs", TP),
        P("fs", TP),
        P(None, TP),
        P(None, TP),
        P(TP),
        P(TP),
        P(TP, "fs"),
        P(),
    )
    out_specs = P(("rep", "fs"), TP, None)
    return jax.shard_map(
        per_device, mesh=split, in_specs=in_specs, out_specs=out_specs, check_vma=False
    )
```

profile of v0, /device:TPU:8, one launch (start us, length us, event | category | flops | bytes accessed | tf_op | source)
XLA Modules:
  0.0 770.2 jit_solution(12787065556506595714)
XLA Ops:
  6.5 1.1 fusion.44
  7.7 1.1 fusion.46
  8.8 13.9 %all-gather = bf16[256,1024]{1,0:T(8,128)(2,1)} all-gather(bf16[64,1024]{1,0:T(8,128)(2,1)S(1)} %get-tuple-element.171), channel_id=2, replica_groups=mesh['rep'=2,'fs'=32,'tp_0'=4,'tp_1'=2] {'tp_0'}, dimensions={0}, use_global_device_ids=true | all-gather | bytes 655360 | tf_op jit(solution)/shard_map/all_gather | solution.py:39
  22.8 2.1 all-gather.1
  28.7 124.4 %all_gather.48 = bf16[256,1024]{0,1:T(8,128)(2,1)} all-gather(bf16[256,32]{0,1:T(8,128)(2,1)S(1)} %copy-done.15), channel_id=1, replica_groups=mesh['rep'=2,'fs'=32,'tp_0'=4,'tp_1'=2] {'fs'}, dimensions={1}, use_global_device_ids=true | all-gather | bytes 540672 | tf_op jit(solution)/shard_map/all_gather | solution.py:214
  153.1 1.3 copy.35
  154.5 1.5 pad_maximum_fusion
  156.0 151.1 %all-gather.21.cloned.1.call-done = bf16[786432]{0:T(1024)(128)(2,1)} async-done(((bf16[24576]{0:T(1024)(128)(2,1)}), bf16[786432]{0:T(1024)(128)(2,1)}) %all-gather.21.cloned.1.call-update) | async-done | bytes 1572880 | tf_op jit(solution)/shard_map/all_gather | solution.py:23
  307.1 2.7 reshape.445
  310.9 2.1 fusion.99
  313.9 1.8 convolution_bitcast_fusion.2
  316.5 1.9 fusion.71
  321.0 1.7 convolution_convert_fusion.5
  323.4 1.8 fusion.48
  325.2 1.4 convolution_multiply_fusion.1
  326.6 1.5 fusion.104
  328.1 1.8 convolution_bitcast_fusion.1
  329.9 1.1 broadcast.305.clone.1
  331.0 13.0 %while.26 = (s32[]{:T(128)}, f32[1,128,256]{2,1,0:T(8,128)S(1)}, f32[8,1,128,256]{3,2,1,0:T(8,128)}, f32[1]{0:T(128)}, f32[8,1,128,256]{3,2,1,0:T(8,128)}, /*index=5*/s32[]{:T(128)}, s32[]{:T(128)}) while((s32[]{:T(128)}, f32[1,128,256]{2,1,0:T(8,128)S(1)}, f32[8,1,128,256]{3,2,1,0:T(8,128)}, f32[1]{0:T(128)}, ...), condition=%wide.region_2.3_spmd.clone, body=%wide.region_1.2_spmd.clone.sunk | while | flops 131075 | bytes 655968 | solution.py:124
  344.0 3.5 reverse.11
  347.6 2.9 reverse.10
  350.5 1.1 copy.48
  351.9 1.6 fusion.105
  353.4 1.8 convolution_bitcast_fusion
  355.2 1.1 broadcast.305.clone
  356.3 13.0 %while.27 = (s32[]{:T(128)}, f32[1,128,256]{2,1,0:T(8,128)S(1)}, f32[8,1,128,256]{3,2,1,0:T(8,128)}, f32[1]{0:T(128)}, f32[8,1,128,256]{3,2,1,0:T(8,128)}, /*index=5*/s32[]{:T(128)}, s32[]{:T(128)}) while((s32[]{:T(128)}, f32[1,128,256]{2,1,0:T(8,128)S(1)}, f32[8,1,128,256]{3,2,1,0:T(8,128)}, f32[1]{0:T(128)}, ...), condition=%wide.region_4.5_spmd.clone, body=%wide.region_3.4_spmd.clone.sunk | while | flops 131075 | bytes 655968 | solution.py:124
  369.3 3.3 convolution_add_fusion
  372.7 9.0 %rev.2 = f32[1024,1,256]{2,0,1:T(8,128)} reverse(f32[1024,1,256]{2,0,1:T(8,128)} %bitcast.150), dimensions={0} | reverse | bytes 2097152 | tf_op jit(solution)/shard_map/rev | solution.py:138
  381.6 2.4 convolution_add_fusion.1
  384.7 2.1 reshape_reshape.24
  386.8 4.7 convolution_convert_fusion.1
  393.2 38.3 %reduce-scatter.3.cloned.1.call-done = bf16[128,1024]{1,0:T(8,128)(2,1)} async-done(((bf16[1024,1024]{1,0:T(8,128)(2,1)}), bf16[128,1024]{1,0:T(8,128)(2,1)}) %reduce-scatter.3.cloned.1.call-update) | async-done | bytes 262160 | tf_op jit(solution)/shard_map/reduce_scatter | solution.py:65
  431.5 1.1 fusion.36
  432.6 1.2 fusion.40
  434.0 13.7 %all-gather.3 = bf16[256,1024]{1,0:T(8,128)(2,1)} all-gather(bf16[64,1024]{1,0:T(8,128)(2,1)S(1)} %get-tuple-element.167), channel_id=5, replica_groups=mesh['rep'=2,'fs'=32,'tp_0'=4,'tp_1'=2] {'tp_0'}, dimensions={0}, use_global_device_ids=true | all-gather | bytes 655360 | tf_op jit(solution)/shard_map/all_gather | solution.py:39
  447.8 122.5 %all_gather.55 = bf16[352,1024]{0,1:T(8,128)(2,1)} all-gather(bf16[352,32]{0,1:T(8,128)(2,1)S(1)} %copy-done.12), channel_id=1, replica_groups=mesh['rep'=2,'fs'=32,'tp_0'=4,'tp_1'=2] {'fs'}, dimensions={1}, use_global_device_ids=true | all-gather | bytes 743424 | tf_op jit(solution)/shard_map/all_gather | solution.py:239
  570.4 84.3 %all-gather.23.cloned.1.call-done = bf16[720896]{0:T(1024)(128)(2,1)} async-done(((bf16[22528]{0:T(1024)(128)(2,1)}), bf16[720896]{0:T(1024)(128)(2,1)}) %all-gather.23.cloned.1.call-update) | async-done | bytes 1441808 | tf_op jit(solution)/shard_map/all_gather | solution.py:23
  654.7 1.7 reshape.448
  656.5 2.1 all-gather.4
  658.8 2.1 reshape_reshape.26
  660.8 2.1 reshape_reshape.25
  662.9 11.5 %all-gather.17.cloned.1.call-done = bf16[8,64,1024]{2,1,0:T(8,128)(2,1)} async-done(((bf16[4,64,1024]{2,1,0:T(8,128)(2,1)}), bf16[8,64,1024]{2,1,0:T(8,128)(2,1)}) %all-gather.17.cloned.1.call-update) | async-done | bytes 1048592 | tf_op jit(solution)/shard_map/all_gather | solution.py:39
  674.4 1.3 copy.46
  675.8 33.9 %all-gather.19.cloned.1.call-done = bf16[8,64,1024]{2,1,0:T(8,128)(2,1)} async-done(((bf16[2,64,1024]{2,1,0:T(8,128)(2,1)}), bf16[8,64,1024]{2,1,0:T(8,128)(2,1)}) %all-gather.19.cloned.1.call-update) | async-done | bytes 1048592 | tf_op jit(solution)/shard_map/all_gather | solution.py:39
  709.6 1.5 pad_maximum_fusion.1
  713.5 4.8 convolution_convert_fusion
  718.3 42.1 %reduce-scatter.5.cloned.1.call-done = bf16[128,1024]{1,0:T(8,128)(2,1)} async-done(((bf16[1024,1024]{1,0:T(8,128)(2,1)}), bf16[128,1024]{1,0:T(8,128)(2,1)}) %reduce-scatter.5.cloned.1.call-update) | async-done | bytes 262160 | tf_op jit(solution)/shard_map/reduce_scatter | solution.py:65
  761.5 1.8 fusion.74
  (146 shorter events, 40.4 us)
Async XLA Ops:
  6.5 146.6 %all-gather.13.cloned.1.call-start = ((), (), s32[]{:S(2)}) async-start(), calls=%async_computation.2 | async-start | bytes 1572864 | tf_op jit(solution)/shard_map/all_gather | solution.py:39
  7.6 17.4 %copy-start.16 = (bf16[32,256]{1,0:T(8,128)(2,1)S(1)}, bf16[32,256]{1,0:T(8,128)(2,1)}, u32[]{:S(2)}) copy-start(bf16[32,256]{1,0:T(8,128)(2,1)} %param.26) | copy-start | bytes 49156
  7.6 17.4 %copy-start.17 = (bf16[32,256]{1,0:T(8,128)(2,1)S(1)}, bf16[32,256]{1,0:T(8,128)(2,1)}, u32[]{:S(2)}) copy-start(bf16[32,256]{1,0:T(8,128)(2,1)} %param.27) | copy-start | bytes 49156
  7.7 17.4 %copy-start.18 = (bf16[32,128]{1,0:T(8,128)(2,1)S(1)}, bf16[32,128]{1,0:T(8,128)(2,1)}, u32[]{:S(2)}) copy-start(bf16[32,128]{1,0:T(8,128)(2,1)} %param.25) | copy-start | bytes 24580
  7.7 17.4 %copy-start.19 = (bf16[32,128]{1,0:T(8,128)(2,1)S(1)}, bf16[32,128]{1,0:T(8,128)(2,1)}, u32[]{:S(2)}) copy-start(bf16[32,128]{1,0:T(8,128)(2,1)} %param.24) | copy-start | bytes 24580
  7.7 18.1 %copy-start.25 = (f32[2,1]{0,1:T(1,128)S(1)}, f32[2,1]{0,1:T(1,128)}, u32[]{:S(2)}) copy-start(f32[2,1]{0,1:T(1,128)} %param.28) | copy-start | bytes 28
  8.8 19.9 %copy-start.15 = (bf16[256,32]{0,1:T(8,128)(2,1)S(1)}, bf16[256,32]{0,1:T(8,128)(2,1)}, u32[]{:S(2)}) copy-start(bf16[256,32]{0,1:T(8,128)(2,1)} %param.29) | copy-start | bytes 49156
  22.7 131.7 %all-gather.15.cloned.1.call-start = ((), (), s32[]{:S(2)}) async-start(), calls=%async_computation.3 | async-start | bytes 1310720 | tf_op jit(solution)/shard_map/all_gather | solution.py:39
  24.9 282.1 %all-gather.21.cloned.1.call-start = ((), (), s32[]{:S(2)}) async-start(), calls=%async_computation.8 | async-start | bytes 1622016 | tf_op jit(solution)/shard_map/all_gather | solution.py:23
  25.7 405.7 %reduce-scatter.3.cloned.1.call-start = ((), (), s32[]{:S(2)}) async-start(), calls=%async_computation.4 | async-start | bytes 2359296 | tf_op jit(solution)/shard_map/reduce_scatter | solution.py:65
  325.2 2.9 copy-start.3
  325.2 2.9 copy-start.4
  331.0 16.6 %copy-start.7 = (bf16[1024,128]{0,1:T(8,128)(2,1)S(1)}, bf16[1024,128]{0,1:T(8,128)(2,1)}, u32[]{:S(2)}) copy-start(bf16[1024,128]{0,1:T(8,128)(2,1)} %get-tuple-element.170) | copy-start | bytes 786436
  344.0 7.6 copy-start.11
  355.2 14.1 %copy-start.1 = (f32[8,256,128]{1,2,0:T(8,128)S(1)}, f32[8,256,128]{1,2,0:T(8,128)}, u32[]{:S(2)}) copy-start(f32[8,256,128]{1,2,0:T(8,128)} %fusion.105) | copy-start | bytes 3145732
  372.7 9.0 %copy-start = (f32[8,256,128]{1,2,0:T(8,128)S(1)}, f32[8,256,128]{1,2,0:T(8,128)}, u32[]{:S(2)}) copy-start(f32[8,256,128]{1,2,0:T(8,128)} %fusion.104) | copy-start | bytes 3145732
  372.7 9.0 %copy-start.6 = (bf16[1024,1,128]{2,0,1:T(8,128)(2,1)S(1)}, bf16[1024,1,128]{2,0,1:T(8,128)(2,1)}, u32[]{:S(2)}) copy-start(bf16[1024,1,128]{2,0,1:T(8,128)(2,1)} %copy.47) | copy-start | bytes 786436
  381.6 2.5 copy-start.2
  391.5 0.7 copy-start.13
  391.5 0.8 copy-start.14
  391.5 41.0 %copy-start.5 = (bf16[1,128,1024]{2,1,0:T(8,128)(2,1)S(1)}, bf16[1,128,1024]{2,1,0:T(8,128)(2,1)}, u32[]{:S(2)}) copy-start(bf16[1,128,1024]{2,1,0:T(8,128)(2,1)} %param.22) | copy-start | bytes 786436
  391.5 41.0 %copy-start.20 = (f32[1024]{0:T(1024)S(1)}, f32[1024]{0:T(1024)}, u32[]{:S(2)}) copy-start(f32[1024]{0:T(1024)} %param.30) | copy-start | bytes 12292
  391.5 42.3 %copy-start.21 = (f32[1024]{0:T(1024)S(1)}, f32[1024]{0:T(1024)}, u32[]{:S(2)}) copy-start(f32[1024]{0:T(1024)} %param.31) | copy-start | bytes 12292
  391.6 263.1 %all-gather.23.cloned.1.call-start = ((), (), s32[]{:S(2)}) async-start(), calls=%async_computation.9 | async-start | bytes 1486848 | tf_op jit(solution)/shard_map/all_gather | solution.py:23
  393.1 281.3 %all-gather.17.cloned.1.call-start = ((), (), s32[]{:S(2)}) async-start(), calls=%async_computation.5 | async-start | bytes 1572864 | tf_op jit(solution)/shard_map/all_gather | solution.py:39
  432.6 15.2 %copy-start.23 = (f32[3,352]{1,0:T(4,128)S(1)}, f32[3,352]{1,0:T(4,128)}, u32[]{:S(2)}) copy-start(f32[3,352]{1,0:T(4,128)} %param.35) | copy-start | bytes 12676
  432.6 15.2 %copy-start.24 = (f32[3,352]{1,0:T(4,128)S(1)}, f32[3,352]{1,0:T(4,128)}, u32[]{:S(2)}) copy-start(f32[3,352]{1,0:T(4,128)} %param.34) | copy-start | bytes 12676
  432.6 15.2 %copy-start.12 = (bf16[352,32]{0,1:T(8,128)(2,1)S(1)}, bf16[352,32]{0,1:T(8,128)(2,1)}, u32[]{:S(2)}) copy-start(bf16[352,32]{0,1:T(8,128)(2,1)} %param.38) | copy-start | bytes 67588
  447.7 261.9 %all-gather.19.cloned.1.call-start = ((), (), s32[]{:S(2)}) async-start(), calls=%async_computation.6 | async-start | bytes 1310720 | tf_op jit(solution)/shard_map/all_gather | solution.py:39
  658.6 101.8 %reduce-scatter.5.cloned.1.call-start = ((), (), s32[]{:S(2)}) async-start(), calls=%async_computation.7 | async-start | bytes 2359296 | tf_op jit(solution)/shard_map/reduce_scatter | solution.py:65
  709.6 1.5 copy-start.9
  711.2 1.1 copy-start.10
  712.3 1.1 copy-start.8
  712.3 1.1 copy-start.26
  712.3 1.1 copy-start.27
  718.3 43.3 %copy-start.22 = (f32[1024]{0:T(1024)S(1)}, f32[1024]{0:T(1024)}, u32[]{:S(2)}) copy-start(f32[1024]{0:T(1024)} %param.39) | copy-start | bytes 12292
Sparse Core Ops, SparseCore 0:
  22.9 23.9 all-gather.12
  48.9 33.0 all-gather.14
  84.1 222.8 all-gather.20
  391.7 39.7 reduce-scatter.2
  433.4 221.2 all-gather.22
  656.7 17.7 all-gather.16
  676.5 33.0 all-gather.18
  718.4 41.9 reduce-scatter.4
where the time goes:
time: 772 us; the launch traced here: 770 us
  waiting for transfers between devices  361 us (47%)
  blocking collectives  279 us (36%)
  other arithmetic  43.4 us (6%)
  local copies, waits for them, and re-layouts  40.7 us (5%)
  matrix products  29.9 us (4%)
  between operations  15.5 us (2%)
    all_gather x2, waiting for transfers between devices, gather_together(): lines, at, gathered = (lax.all_gather(flat, axis), 0, [])  235 us
    all_gather x1, blocking collectives, per_device(): output_columns = lax.all_gather(mixer_output, 'fs', axis=1, tiled=True)  124 us
    all_gather x1, blocking collectives, per_device(): down_columns = lax.all_gather(down_weight, 'fs', axis=1, tiled=True)  123 us
    reduce_scatter x2, waiting for transfers between devices, own_rows_2(): lax.psum_scatter(everything.astype(jnp.bfloat16), axis, scatter_dimension...  80.4 us
    all_gather x4, waiting for transfers between devices, all_blocks(): pieces = lax.all_gather(pieces, axes[k], axis=0, tiled=True)  45.4 us
    all_gather x4, blocking collectives, all_blocks(): pieces = lax.all_gather(pieces, axes[k], axis=0, tiled=True)  31.8 us
  transfers between devices with their start and end apart: 8, of which 6 were waited for; matrix products, arithmetic and copies ran while one was open for 2% of the time, Pallas kernels for 0%

commit v1 on v0

--- a/solution.py
+++ b/solution.py
@@ -10,6 +10,13 @@
 TP = ("tp_0", "tp_1")
 epsilon = 1e-06
 rope_base = 10000.0
+
+
+def all_by_exchange(x, mesh_axis, dim):
+    devices = lax.axis_size(mesh_axis)
+    pieces = jnp.stack([x for _ in range(devices)])
+    pieces = lax.all_to_all(pieces, mesh_axis, split_axis=0, concat_axis=0)
+    return jnp.concatenate(pieces, axis=dim)
 
 
 def joined_along(pieces, dim):
@@ -36,7 +43,7 @@
 def all_blocks(value, axes, order):
     pieces = value[None]
     for k in order:
-        pieces = lax.all_gather(pieces, axes[k], axis=0, tiled=True)
+        pieces = all_by_exchange(pieces, axes[k], 0)
     carried = [lax.axis_size(axes[k]) for k in reversed(order)]
     pieces = pieces.reshape(*carried, *value.shape)
     turned = sorted(range(len(order)), key=lambda place: order[len(order) - 1 - place])

time: 772 us -> 677 us (0.88)
  the two profiles are of different devices: /device:TPU:8 before, /device:TPU:16 now
where the time goes in v1:
time: 677 us; the launch traced here: 675 us
  waiting for transfers between devices  257 us (38%)
  blocking collectives  254 us (38%)
  local copies, waits for them, and re-layouts  49.9 us (7%)
  other arithmetic  44.9 us (7%)
  matrix products  29.8 us (4%)
  starting transfers between devices  23.4 us (3%)
  between operations  15.2 us (2%)
    all_gather x2, waiting for transfers between devices, gather_together(): lines, at, gathered = (lax.all_gather(flat, axis), 0, [])  144 us
    all_gather x1, blocking collectives, per_device(): output_columns = lax.all_gather(mixer_output, 'fs', axis=1, tiled=True)  123 us
    all_gather x1, blocking collectives, per_device(): down_columns = lax.all_gather(down_weight, 'fs', axis=1, tiled=True)  122 us
    reduce_scatter x2, waiting for transfers between devices, own_rows_2(): lax.psum_scatter(everything.astype(jnp.bfloat16), axis, scatter_dimension...  94.2 us
    all_to_all x6, starting transfers between devices, all_by_exchange(): pieces = lax.all_to_all(pieces, mesh_axis, split_axis=0, concat_axis=0)  23.3 us
    all_to_all x6, waiting for transfers between devices, all_by_exchange(): pieces = lax.all_to_all(pieces, mesh_axis, split_axis=0, concat_axis=0)  18.5 us
    add x16, other arithmetic, advance(): return (step_decay[:, None, None] * carried + update, carried)  15.1 us
  transfers between devices with their start and end apart: 10, of which 8 were waited for; matrix products, arithmetic and copies ran while one was open for 3% of the time, Pallas kernels for 0%

profile of v1, /device:TPU:16, one launch (start us, length us, event | category | flops | bytes accessed | tf_op | source)
XLA Modules:
  0.0 674.7 jit_solution(8814025345174910351)
XLA Ops:
  8.0 1.3 pad_maximum_fusion.7
  12.4 4.3 all-to-all-start
  19.6 6.6 all-to-all-done
  26.2 3.4 all-to-all-start.2
  29.7 1.4 all-to-all-done.2
  31.2 4.6 all_to_all.40
  36.9 3.6 all-to-all-start.3
  41.8 123.3 %all_gather.20 = bf16[256,1024]{0,1:T(8,128)(2,1)} all-gather(bf16[256,32]{0,1:T(8,128)(2,1)S(1)} %copy-done.18), channel_id=1, replica_groups=mesh['rep'=2,'fs'=32,'tp_0'=4,'tp_1'=2] {'fs'}, dimensions={1}, use_global_device_ids=true | all-gather | bytes 540672 | tf_op jit(solution)/shard_map/all_gather | solution.py:221
  166.2 1.5 pad_maximum_fusion
  167.7 59.6 %all-gather.5.cloned.1.call-done = bf16[786432]{0:T(1024)(128)(2,1)} async-done(((bf16[24576]{0:T(1024)(128)(2,1)}), bf16[786432]{0:T(1024)(128)(2,1)}) %all-gather.5.cloned.1.call-update) | async-done | bytes 1572880 | tf_op jit(solution)/shard_map/all_gather | solution.py:30
  227.4 2.7 reshape.443
  231.1 2.1 fusion.99
  234.2 1.8 convolution_bitcast_fusion.2
  236.8 1.9 fusion.71
  241.4 1.7 convolution_convert_fusion.5
  243.8 1.8 fusion.48
  245.5 1.4 convolution_multiply_fusion.1
  246.9 1.6 fusion.104
  248.5 1.8 convolution_bitcast_fusion.1
  251.4 13.0 %while.26 = (s32[]{:T(128)}, f32[1,128,256]{2,1,0:T(8,128)S(1)}, f32[8,1,128,256]{3,2,1,0:T(8,128)}, f32[1]{0:T(128)}, f32[8,1,128,256]{3,2,1,0:T(8,128)}, /*index=5*/s32[]{:T(128)}, s32[]{:T(128)}) while((s32[]{:T(128)}, f32[1,128,256]{2,1,0:T(8,128)S(1)}, f32[8,1,128,256]{3,2,1,0:T(8,128)}, f32[1]{0:T(128)}, ...), condition=%wide.region_2.3_spmd.clone, body=%wide.region_1.2_spmd.clone.sunk | while | flops 131075 | bytes 655968 | solution.py:131
  264.4 3.5 reverse.11
  268.0 2.9 reverse.10
  272.3 1.5 fusion.105
  273.8 1.8 convolution_bitcast_fusion
  276.6 13.0 %while.27 = (s32[]{:T(128)}, f32[1,128,256]{2,1,0:T(8,128)S(1)}, f32[8,1,128,256]{3,2,1,0:T(8,128)}, f32[1]{0:T(128)}, f32[8,1,128,256]{3,2,1,0:T(8,128)}, /*index=5*/s32[]{:T(128)}, s32[]{:T(128)}) while((s32[]{:T(128)}, f32[1,128,256]{2,1,0:T(8,128)S(1)}, f32[8,1,128,256]{3,2,1,0:T(8,128)}, f32[1]{0:T(128)}, ...), condition=%wide.region_4.5_spmd.clone, body=%wide.region_3.4_spmd.clone.sunk | while | flops 131075 | bytes 655968 | solution.py:131
  289.7 3.4 convolution_add_fusion
  293.0 9.0 %rev.2 = f32[1024,1,256]{2,0,1:T(8,128)} reverse(f32[1024,1,256]{2,0,1:T(8,128)} %bitcast.154), dimensions={0} | reverse | bytes 2097152 | tf_op jit(solution)/shard_map/rev | solution.py:145
  302.0 2.4 convolution_add_fusion.1
  305.1 2.1 reshape_reshape.24
  307.2 4.7 convolution_convert_fusion.1
  314.2 46.9 %reduce-scatter.3.cloned.1.call-done = bf16[128,1024]{1,0:T(8,128)(2,1)} async-done(((bf16[1024,1024]{1,0:T(8,128)(2,1)}), bf16[128,1024]{1,0:T(8,128)(2,1)}) %reduce-scatter.3.cloned.1.call-update) | async-done | bytes 262160 | tf_op jit(solution)/shard_map/reduce_scatter | solution.py:72
  362.1 1.2 fusion.40
  365.1 3.5 all-to-all-start.4
  368.6 121.7 %all_gather.23 = bf16[352,1024]{0,1:T(8,128)(2,1)} all-gather(bf16[352,32]{0,1:T(8,128)(2,1)S(1)} %copy-done.15), channel_id=1, replica_groups=mesh['rep'=2,'fs'=32,'tp_0'=4,'tp_1'=2] {'fs'}, dimensions={1}, use_global_device_ids=true | all-gather | bytes 743424 | tf_op jit(solution)/shard_map/all_gather | solution.py:246
  490.3 84.7 %all-gather.7.cloned.1.call-done = bf16[720896]{0:T(1024)(128)(2,1)} async-done(((bf16[22528]{0:T(1024)(128)(2,1)}), bf16[720896]{0:T(1024)(128)(2,1)}) %all-gather.7.cloned.1.call-update) | async-done | bytes 1441808 | tf_op jit(solution)/shard_map/all_gather | solution.py:30
  575.0 1.7 reshape.444
  577.5 4.1 all-to-all-start.6
  581.7 1.6 all-to-all-done.6
  583.3 4.6 all_to_all.41
  587.8 2.1 stack.31
  589.9 4.4 all-to-all-start.7
  594.3 1.2 fusion.100
  595.5 3.1 reshape_reshape.26
  598.7 2.1 reshape_reshape.25
  600.8 8.9 %all-to-all-done.7 = bf16[4,2,64,1024]{3,2,1,0:T(8,128)(2,1)S(1)} async-done(((bf16[4,2,64,1024]{3,2,1,0:T(8,128)(2,1)}), bf16[4,2,64,1024]{3,2,1,0:T(8,128)(2,1)S(1)}, u32[]{:S(2)}, u32[]{:S(2)}) %all-to-all-start.7) | async-done | bytes 1048608 | tf_op jit(solution)/shard_map/all_to_all | solution.py:18
  613.1 4.7 convolution_convert_fusion
  617.9 47.4 %reduce-scatter.5.cloned.1.call-done = bf16[128,1024]{1,0:T(8,128)(2,1)} async-done(((bf16[1024,1024]{1,0:T(8,128)(2,1)}), bf16[128,1024]{1,0:T(8,128)(2,1)}) %reduce-scatter.5.cloned.1.call-update) | async-done | bytes 262160 | tf_op jit(solution)/shard_map/reduce_scatter | solution.py:72
  666.4 1.8 fusion.74
  (158 shorter events, 55.8 us)
Async XLA Ops:
  6.5 220.8 %all-gather.5.cloned.1.call-start = ((), (), s32[]{:S(2)}) async-start(), calls=%async_computation.12 | async-start | bytes 1622016 | tf_op jit(solution)/shard_map/all_gather | solution.py:30
  10.4 6.3 copy-start.24
  12.4 13.8 %all-to-all-start = ((bf16[4,1,64,1024]{3,2,1,0:T(8,128)(2,1)}), bf16[4,1,64,1024]{3,2,1,0:T(8,128)(2,1)S(1)}, u32[]{:S(2)}, u32[]{:S(2)}) async-start(bf16[4,1,64,1024]{3,2,1,0:T(8,128)(2,1)} %stack.24), calls=%async_computation | async-start | bytes 1048576 | tf_op jit(solution)/shard_map/all_to_all | solution.py:18
  26.2 5.0 all-to-all-start.2
  36.9 4.9 copy-start.18
  36.9 129.3 %all-to-all-start.3 = ((bf16[4,2,64,1024]{3,2,1,0:T(8,128)(2,1)}), bf16[4,2,64,1024]{3,2,1,0:T(8,128)(2,1)S(1)}, u32[]{:S(2)}, u32[]{:S(2)}) async-start(bf16[4,2,64,1024]{3,2,1,0:T(8,128)(2,1)} %stack.27), calls=%async_computation.3 | async-start | bytes 2097152 | tf_op jit(solution)/shard_map/all_to_all | solution.py:18
  40.5 320.5 %reduce-scatter.3.cloned.1.call-start = ((), (), s32[]{:S(2)}) async-start(), calls=%async_computation.10 | async-start | bytes 2359296 | tf_op jit(solution)/shard_map/reduce_scatter | solution.py:72
  235.9 0.8 copy-start.28
  245.5 3.0 copy-start.3
  245.5 3.0 copy-start.4
  251.4 16.6 %copy-start.11 = (bf16[1024,128]{0,1:T(8,128)(2,1)S(1)}, bf16[1024,128]{0,1:T(8,128)(2,1)}, u32[]{:S(2)}) copy-start(bf16[1024,128]{0,1:T(8,128)(2,1)} %get-tuple-element.170) | copy-start | bytes 786436
  272.0 1.8 copy-start.6
  272.0 1.8 copy-start.27
  275.6 14.1 %copy-start.1 = (f32[8,256,128]{1,2,0:T(8,128)S(1)}, f32[8,256,128]{1,2,0:T(8,128)}, u32[]{:S(2)}) copy-start(f32[8,256,128]{1,2,0:T(8,128)} %fusion.105) | copy-start | bytes 3145732
  293.0 9.0 %copy-start = (f32[8,256,128]{1,2,0:T(8,128)S(1)}, f32[8,256,128]{1,2,0:T(8,128)}, u32[]{:S(2)}) copy-start(f32[8,256,128]{1,2,0:T(8,128)} %fusion.104) | copy-start | bytes 3145732
  293.0 9.0 %copy-start.8 = (bf16[1024,1,128]{2,0,1:T(8,128)(2,1)S(1)}, bf16[1024,1,128]{2,0,1:T(8,128)(2,1)}, u32[]{:S(2)}) copy-start(bf16[1024,1,128]{2,0,1:T(8,128)(2,1)} %copy.43) | copy-start | bytes 786436
  302.0 2.5 copy-start.2
  311.9 0.7 copy-start.16
  311.9 0.8 copy-start.17
  311.9 1.6 copy-start.22
  311.9 1.6 copy-start.23
  311.9 50.2 %copy-start.7 = (bf16[1,128,1024]{2,1,0:T(8,128)(2,1)S(1)}, bf16[1,128,1024]{2,1,0:T(8,128)(2,1)}, u32[]{:S(2)}) copy-start(bf16[1,128,1024]{2,1,0:T(8,128)(2,1)} %param.22) | copy-start | bytes 786436
  312.0 50.2 %copy-start.19 = (f32[1024]{0:T(1024)S(1)}, f32[1024]{0:T(1024)}, u32[]{:S(2)}) copy-start(f32[1024]{0:T(1024)} %param.30) | copy-start | bytes 12292
  312.0 52.1 %copy-start.20 = (f32[1024]{0:T(1024)S(1)}, f32[1024]{0:T(1024)}, u32[]{:S(2)}) copy-start(f32[1024]{0:T(1024)} %param.31) | copy-start | bytes 12292
  312.0 263.0 %all-gather.7.cloned.1.call-start = ((), (), s32[]{:S(2)}) async-start(), calls=%async_computation.13 | async-start | bytes 1486848 | tf_op jit(solution)/shard_map/all_gather | solution.py:30
  363.4 0.7 copy-start.9
  363.4 5.2 copy-start.15
  365.1 212.4 %all-to-all-start.4 = ((bf16[4,1,64,1024]{3,2,1,0:T(8,128)(2,1)}), bf16[4,1,64,1024]{3,2,1,0:T(8,128)(2,1)S(1)}, u32[]{:S(2)}, u32[]{:S(2)}) async-start(bf16[4,1,64,1024]{3,2,1,0:T(8,128)(2,1)} %stack.28), calls=%async_computation.5 | async-start | bytes 1048576 | tf_op jit(solution)/shard_map/all_to_all | solution.py:18
  577.5 5.8 all-to-all-start.6
  589.9 19.8 %all-to-all-start.7 = ((bf16[4,2,64,1024]{3,2,1,0:T(8,128)(2,1)}), bf16[4,2,64,1024]{3,2,1,0:T(8,128)(2,1)S(1)}, u32[]{:S(2)}, u32[]{:S(2)}) async-start(bf16[4,2,64,1024]{3,2,1,0:T(8,128)(2,1)} %stack.31), calls=%async_computation.8 | async-start | bytes 2097152 | tf_op jit(solution)/shard_map/all_to_all | solution.py:18
  594.3 71.0 %reduce-scatter.5.cloned.1.call-start = ((), (), s32[]{:S(2)}) async-start(), calls=%async_computation.11 | async-start | bytes 2359296 | tf_op jit(solution)/shard_map/reduce_scatter | solution.py:72
  595.5 3.1 copy-start.5
  609.7 1.1 copy-start.13
  610.8 1.1 copy-start.14
  612.0 1.1 copy-start.12
  612.0 1.1 copy-start.25
  612.0 1.1 copy-start.26
  612.0 1.1 copy-start.29
  612.0 1.1 copy-start.30
  617.9 48.5 %copy-start.10 = (bf16[128,1024]{1,0:T(8,128)(2,1)S(1)}, bf16[128,1024]{1,0:T(8,128)(2,1)}, u32[]{:S(2)}) copy-start(bf16[128,1024]{1,0:T(8,128)(2,1)} %copy-done.9) | copy-start | bytes 786436
  617.9 48.5 %copy-start.21 = (f32[1024]{0:T(1024)S(1)}, f32[1024]{0:T(1024)}, u32[]{:S(2)}) copy-start(f32[1024]{0:T(1024)} %param.39) | copy-start | bytes 12292
Sparse Core Ops, SparseCore 0:
  9.5 217.8 all-gather.4
  312.1 48.8 reduce-scatter.2
  363.1 211.8 all-gather.6
  618.0 47.2 reduce-scatter.4
